TPU v7x, 32 devices: a whole 2x2x4 slice. The times are simulated.
32 devices in a mesh: fs: 16 (over z, y, x), tp: 2 (over core).
Axes of the slice: x: 2, y: 2, z: 4, core: 2. Of those that a mesh axis runs over, the one named last changes fastest.
Arguments:
- residual_in: bfloat16 [4096, 2048], P(('fs', 'tp')), may hold values from -6 to 6
- gain_first: float32 [2048], replicated, may hold values from 0.1 to 1.9
- gain_mixer: float32 [2048], replicated, may hold values from 0.1 to 1.9
- gain_second: float32 [2048], replicated, may hold values from 0.1 to 1.9
- gate_weight: float32 [2048, 6144], P('fs', 'tp'), may hold values from -0.125 to 0.125
- gate_scale: float32 [6144], P('tp'), may hold values from 0.3 to 3
- up_weight: float32 [2048, 6144], P('fs', 'tp'), may hold values from -0.125 to 0.125
- up_scale: float32 [6144], P('tp'), may hold values from 0.3 to 3
- down_weight: float32 [6144, 2048], P('tp', 'fs'), may hold values from -0.078125 to 0.078125
- down_scale: float32 [2048], P('fs'), may hold values from 0.3 to 3
- query_weight: float32 [2048, 2048], P('fs', 'tp'), may hold values from -0.125 to 0.125
- query_scale: float32 [2048], P('tp'), may hold values from 0.3 to 3
- key_weight: float32 [2048, 2048], P('fs', 'tp'), may hold values from -0.125 to 0.125
- key_scale: float32 [2048], P('tp'), may hold values from 0.3 to 3
- value_weight: float32 [2048, 2048], P('fs', 'tp'), may hold values from -0.125 to 0.125
- value_scale: float32 [2048], P('tp'), may hold values from 0.3 to 3
- output_weight: float32 [2048, 2048], P('tp', 'fs'), may hold values from -0.125 to 0.125
- output_scale: float32 [2048], P('fs'), may hold values from 0.3 to 3
Outputs:
- residual_out: bfloat16 [4096, 2048], P(('fs', 'tp'))
All inputs are finite; a program needn't handle non-finite values.
Results may differ from a plain program's by a relative error of at most 0.028.
Values may be sent and summed in bfloat16 or wider, within the bound.
A program may use at most 128 MiB of HBM per device.

v0:
```python
import jax
import jax.numpy as jnp
from jax import lax
from jax.sharding import PartitionSpec as P

HEADS = 8
HEAD_DIM = 256
BLOCK = 64
EPSILON = 1e-06
HEAD_FLOOR = 0.25
ROTARY_BASE = 10000.0
HIGHEST = lax.Precision.HIGHEST


def normalize(sequence_rows, gain_vector):
    values = sequence_rows.astype(jnp.float32)
    scaled = values * lax.rsqrt(jnp.mean(values * values, axis=-1, keepdims=True) + EPSILON)
    return (scaled * gain_vector).astype(jnp.bfloat16)


def collect_rows(sequence_rows, gain_vector):
    return lax.all_gather(normalize(sequence_rows, gain_vector), "tp", axis=0, tiled=True)


def return_rows(inputs, weight, factor):
    term = jnp.dot(inputs, weight, preferred_element_type=jnp.float32) * factor
    return lax.psum_scatter(
        lax.optimization_barrier(term.astype(jnp.bfloat16))
        .astype(jnp.float32)
        .astype(jnp.bfloat16),
        "tp",
        scatter_dimension=0,
        tiled=True,
    ).astype(jnp.float32)


def head_rates(first_head, head_count, length):
    head_number = (first_head + jnp.arange(head_count)).astype(jnp.float32)
    return jnp.exp(jnp.log(1.0 / 16.0) + head_number / (HEADS - 1) * jnp.log(4.0 / length))


def rotate(values, positions):
    half_width = values.shape[-1] // 2
    frequency = ROTARY_BASE ** (-jnp.arange(half_width, dtype=jnp.float32) * 2.0 / values.shape[-1])
    angles = positions[:, None] * frequency[None, :]
    cosine = jnp.cos(angles)[:, None, :]
    sine_value = jnp.sin(angles)[:, None, :]
    front_half = values[..., :half_width]
    back_half = values[..., half_width:]
    return jnp.concatenate(
        [
            front_half * cosine - back_half * sine_value,
            back_half * cosine + front_half * sine_value,
        ],
        axis=-1,
    )


def retention(query_pre, key_pre, value_pre, decay_rates):
    length, head_count, head_width = query_pre.shape
    positions = jnp.arange(length, dtype=jnp.float32)
    query_rot = rotate(query_pre, positions).astype(jnp.bfloat16)
    key_rot = rotate(key_pre, positions).astype(jnp.bfloat16)
    value_low = value_pre.astype(jnp.bfloat16)
    blocks = length // BLOCK
    inside = jnp.arange(BLOCK, dtype=jnp.float32)
    distance = inside[:, None] - inside[None, :]
    within = jnp.where(
        distance >= 0, jnp.exp(-decay_rates[:, None, None] * jnp.maximum(distance, 0.0)), 0.0
    ) * head_width ** (-0.5)
    query_blocks = query_rot.reshape(blocks, BLOCK, head_count, head_width)
    key_blocks = key_rot.reshape(blocks, BLOCK, head_count, head_width)
    value_blocks = value_low.reshape(blocks, BLOCK, head_count, head_width)
    scores = jnp.einsum(
        "nihe,njhe->nhij", query_blocks, key_blocks, preferred_element_type=jnp.float32
    )
    weights = (scores * within[None]).astype(jnp.bfloat16)
    inner_part = jnp.einsum(
        "nhij,njhe->nihe", weights, value_blocks, preferred_element_type=jnp.float32
    )
    fading = jnp.exp(-decay_rates[None, :] * (BLOCK - 1.0 - inside[:, None])) * head_width ** (-0.5)
    key_faded = key_blocks.astype(jnp.float32) * fading[None, :, :, None]
    updates = jnp.einsum(
        "njhd,njhe->nhde", key_faded, value_blocks.astype(jnp.float32), precision=HIGHEST
    )
    block_decay = jnp.exp(-decay_rates * BLOCK)

    def advance(memory_state, update):
        return (memory_state * block_decay[:, None, None] + update, memory_state)

    _, before = lax.scan(
        advance, jnp.zeros((head_count, head_width, head_width), jnp.float32), updates
    )
    rising = jnp.exp(-decay_rates[None, :] * (inside[:, None] + 1.0))
    queried = query_blocks.astype(jnp.float32) * rising[None, :, :, None]
    carried_part = jnp.einsum("nihd,nhde->nihe", queried, before, precision=HIGHEST)
    combined = (inner_part + carried_part).reshape(length, head_count, head_width)
    normed = combined * lax.rsqrt(
        jnp.maximum(jnp.mean(combined * combined, axis=-1, keepdims=True), HEAD_FLOOR)
    )
    return normed.astype(jnp.bfloat16).reshape(length, head_count * head_width)


def body(
    residual_in,
    gain_first,
    gain_mixer,
    gain_second,
    gate_weight,
    gate_scale,
    up_weight,
    up_scale,
    down_weight,
    down_scale,
    query_weight,
    query_scale,
    key_weight,
    key_scale,
    value_weight,
    value_scale,
    output_weight,
    output_scale,
):
    gate_part = gate_weight.astype(jnp.bfloat16)
    up_part = up_weight.astype(jnp.bfloat16)
    down_factor, output_factor = (
        lax.all_gather(down_scale, "fs", axis=0, tiled=True),
        lax.all_gather(output_scale, "fs", axis=0, tiled=True),
    )
    first_input = collect_rows(residual_in, gain_first)
    gate_full, up_full = (
        lax.all_gather(gate_part, "fs", axis=0, tiled=True),
        lax.all_gather(up_part, "fs", axis=0, tiled=True),
    )
    gate_pre = jnp.dot(first_input, gate_full, preferred_element_type=jnp.float32)
    up_pre = jnp.dot(first_input, up_full, preferred_element_type=jnp.float32)
    down_full = lax.all_gather(down_weight.astype(jnp.bfloat16), "fs", axis=1, tiled=True)
    hidden_first = (jax.nn.silu(gate_pre * gate_scale) * (up_pre * up_scale)).astype(jnp.bfloat16)
    mlp_first = return_rows(hidden_first, down_full, down_factor)
    middle = (residual_in.astype(jnp.float32) + 0.5 * mlp_first).astype(jnp.bfloat16)
    mixer_input = collect_rows(middle, gain_mixer)
    local_width = query_weight.shape[1]
    projections = (
        query_weight.astype(jnp.bfloat16),
        key_weight.astype(jnp.bfloat16),
        value_weight.astype(jnp.bfloat16),
    )
    pieces = (
        lax.all_gather(projections[0], "fs", axis=0, tiled=True),
        lax.all_gather(projections[1], "fs", axis=0, tiled=True),
        lax.all_gather(projections[2], "fs", axis=0, tiled=True),
    )
    query_pre, key_pre, value_pre = tuple(
        (
            jnp.dot(mixer_input, pieces[member], preferred_element_type=jnp.float32)
            for member in range(3)
        )
    )
    output_full = lax.all_gather(output_weight.astype(jnp.bfloat16), "fs", axis=1, tiled=True)
    length = mixer_input.shape[0]
    heads_local = local_width // HEAD_DIM
    decay_rates = head_rates(lax.axis_index("tp") * heads_local, heads_local, length)
    mixed = retention(
        (query_pre * query_scale).reshape(length, heads_local, HEAD_DIM),
        (key_pre * key_scale).reshape(length, heads_local, HEAD_DIM),
        (value_pre * value_scale).reshape(length, heads_local, HEAD_DIM),
        decay_rates,
    )
    mixer_out = return_rows(mixed, output_full, output_factor)
    second = (middle.astype(jnp.float32) + mixer_out).astype(jnp.bfloat16)
    last_input = collect_rows(second, gain_second)
    gate_last = jnp.dot(last_input, gate_full, preferred_element_type=jnp.float32) * gate_scale
    up_last = jnp.dot(last_input, up_full, preferred_element_type=jnp.float32) * up_scale
    hidden_second = (jax.nn.silu(gate_last) * up_last).astype(jnp.bfloat16)
    mlp_second = return_rows(hidden_second, down_full, down_factor)
    return (second.astype(jnp.float32) + 0.5 * mlp_second).astype(jnp.bfloat16)


def solution(mesh):
    in_specs = (
        P(("fs", "tp"), None),
        P(),
        P(),
        P(),
        P("fs", "tp"),
        P("tp"),
        P("fs", "tp"),
        P("tp"),
        P("tp", "fs"),
        P("fs"),
        P("fs", "tp"),
        P("tp"),
        P("fs", "tp"),
        P("tp"),
        P("fs", "tp"),
        P("tp"),
        P("tp", "fs"),
        P("fs"),
    )
    out_specs = P(("fs", "tp"), None)
    return jax.shard_map(body, mesh=mesh, in_specs=in_specs, out_specs=out_specs, check_vma=False)
```

profile of v0, /device:TPU:0, one launch (start us, length us, event | category | flops | bytes accessed | tf_op | source)
XLA Modules:
  0.0 955.4 jit_solution(6325975038016141110)
XLA Ops:
  6.5 1.3 fusion.12
  7.9 2.0 fusion.14
  10.0 2.4 convert_element_type.119
  12.5 1.0 convert_element_type.120
  13.5 0.0 all-gather.19.cloned.1.call-start
  13.6 2.4 convert_element_type.122
  16.0 43.0 %all-gather = f32[16,1,128]{2,1,0:T(1,128)S(1)} all-gather(f32[1,1,128]{2,1,0:T(1,128)S(1)} %bitcast.58), channel_id=1, replica_groups=mesh['fs'=16,'tp'=2] {'fs'}, dimensions={0}, use_global_device_ids=true | all-gather | bytes 8704 | tf_op jit(solution)/shard_map/all_gather | solution.py:127
  59.0 118.3 %all-gather.15.cloned.1.call-done = bf16[2048,3072]{1,0:T(8,128)(2,1)} async-done(((bf16[128,3072]{1,0:T(8,128)(2,1)}), bf16[2048,3072]{1,0:T(8,128)(2,1)}) %all-gather.15.cloned.1.call-update) | async-done | bytes 12582928 | tf_op jit(solution)/shard_map/all_gather | solution.py:132
  177.3 9.9 %convolution_multiply_fusion.3 = f32[256,3072]{1,0:T(8,128)} fusion(bf16[256,2048]{1,0:T(8,128)(2,1)} %all-gather.13.cloned.1.call-done, bf16[2048,3072]{1,0:T(8,128)(2,1)} %all-gather.15.cloned.1.call-done, f32[3072]{0:T(1024)S(1)} %copy-done.20), kind=kOutput, calls=%fused_computation.7 | convolution fusion | flops 3222011904 | bytes 16789504 | tf_op jit(solution)/shard_map/dot_general | solution.py:135
  187.2 142.5 %all-gather.17.cloned.1.call-done = bf16[2048,3072]{1,0:T(8,128)(2,1)} async-done(((bf16[128,3072]{1,0:T(8,128)(2,1)}), bf16[2048,3072]{1,0:T(8,128)(2,1)}) %all-gather.17.cloned.1.call-update) | async-done | bytes 12582928 | tf_op jit(solution)/shard_map/all_gather | solution.py:133
  329.7 196.2 %all-gather.19.cloned.1.call-done = bf16[3072,2048]{1,0:T(8,128)(2,1)} async-done(((bf16[3072,128]{1,0:T(8,128)(2,1)}), bf16[3072,2048]{1,0:T(8,128)(2,1)}) %all-gather.19.cloned.1.call-update) | async-done | bytes 12582928 | tf_op jit(solution)/shard_map/all_gather | solution.py:137
  525.9 17.1 %fusion.6 = bf16[256,2048]{1,0:T(8,128)(2,1)} fusion(bf16[3072,2048]{1,0:T(8,128)(2,1)} %all-gather.19.cloned.1.call-done, f32[2048]{0:T(1024)S(1)} %bitcast.56, bf16[256,2048]{1,0:T(8,128)(2,1)S(1)} %copy-done.18, bf16[2048,3072]{1,0:T(8,128)(2,1)} %all-gather.17.cloned.1.call-done, f32[256,3072]{1,0:T(8,128)} %convolution_multiply_fusion.3, ...), kind=kOutput, calls=%fused_computation.15 | convolution fusion | flops 6449004544 | bytes 30429184 | tf_op jit(solution)/shard_map/dot_general | solution.py:26
  543.2 0.7 convert_element_type.131
  543.9 0.0 all-gather.21.cloned.1.call-start
  544.0 5.9 reduce-scatter.4.cloned.1.call-done
  549.8 1.3 fusion.16
  551.2 1.0 fusion.18
  552.3 0.8 convert_element_type.132
  553.1 0.7 convert_element_type.128
  553.9 0.7 convert_element_type.138
  554.8 41.1 %all-gather.1 = f32[16,1,128]{2,1,0:T(1,128)S(1)} all-gather(f32[1,1,128]{2,1,0:T(1,128)S(1)} %bitcast.59), channel_id=1, replica_groups=mesh['fs'=16,'tp'=2] {'fs'}, dimensions={0}, use_global_device_ids=true | all-gather | bytes 8704 | tf_op jit(solution)/shard_map/all_gather | solution.py:128
  596.0 0.1 multiply_exponential_fusion.1
  596.1 0.7 select_multiply_fusion
  596.8 1.1 fusion.42
  598.0 31.3 %all-gather.25.cloned.1.call-done = bf16[2048,1024]{1,0:T(8,128)(2,1)} async-done(((bf16[128,1024]{1,0:T(8,128)(2,1)}), bf16[2048,1024]{1,0:T(8,128)(2,1)}) %all-gather.25.cloned.1.call-update) | async-done | bytes 4194320 | tf_op jit(solution)/shard_map/all_gather | solution.py:149
  629.2 9.2 all-gather.21.cloned.1.call-done
  638.4 4.7 convolution_multiply_fusion.8
  643.2 1.7 reshape.230
  644.9 73.1 %all-gather.27.cloned.1.call-done = bf16[2048,1024]{1,0:T(8,128)(2,1)} async-done(((bf16[128,1024]{1,0:T(8,128)(2,1)}), bf16[2048,1024]{1,0:T(8,128)(2,1)}) %all-gather.27.cloned.1.call-update) | async-done | bytes 4194320 | tf_op jit(solution)/shard_map/all_gather | solution.py:150
  718.0 4.7 convolution_multiply_fusion.7
  722.7 2.7 reshape.231
  725.4 69.6 %all-gather.23.cloned.1.call-done = bf16[2048,1024]{1,0:T(8,128)(2,1)} async-done(((bf16[128,1024]{1,0:T(8,128)(2,1)}), bf16[2048,1024]{1,0:T(8,128)(2,1)}) %all-gather.23.cloned.1.call-update) | async-done | bytes 4194320 | tf_op jit(solution)/shard_map/all_gather | solution.py:151
  795.0 4.6 fusion.10
  799.5 1.4 convert_element_type.130
  801.0 1.5 fusion.48
  802.5 0.3 subtract_convert_fusion.1
  802.8 3.9 fusion.27
  806.7 10.4 %while.13 = (s32[]{:T(128)}, f32[4,256,256]{2,1,0:T(8,128)S(1)}, f32[4,4,256,256]{3,2,1,0:T(8,128)}, f32[4,4,256,256]{3,2,1,0:T(8,128)}, s32[]{:T(128)}, /*index=5*/s32[]{:T(128)}, s32[]{:T(128)}) while((s32[]{:T(128)}, f32[4,256,256]{2,1,0:T(8,128)S(1)}, f32[4,4,256,256]{3,2,1,0:T(8,128)}, f32[4,4,256,256]{3,2,1,0:T(8,128)}, ...), condition=%wide.region_4.5_spmd.clone, body=%wide.region_3.4_spmd.clone.sunk | while | flops 1048603 | bytes 5243520 | solution.py:91
  806.7 1.1 bitcast_dynamic-update-slice_fusion.2
  807.8 1.5 bitcast_add_fusion.2
  809.3 1.1 bitcast_dynamic-update-slice_fusion.2
  810.4 1.5 bitcast_add_fusion.2
  811.9 1.1 bitcast_dynamic-update-slice_fusion.2
  813.0 1.5 bitcast_add_fusion.2
  814.5 1.1 bitcast_dynamic-update-slice_fusion.2
  815.7 1.5 bitcast_add_fusion.2
  817.2 5.1 fusion.24
  822.3 1.6 multiply_reduce_fusion
  824.0 0.1 copy.52
  824.1 0.3 mul.482
  824.4 0.2 copy.59
  824.6 0.7 copy.47
  825.3 0.2 copy.58
  825.5 59.4 %all-gather.29.cloned.1.call-done = bf16[1024,2048]{1,0:T(8,128)(2,1)} async-done(((bf16[1024,128]{1,0:T(8,128)(2,1)}), bf16[1024,2048]{1,0:T(8,128)(2,1)}) %all-gather.29.cloned.1.call-update) | async-done | bytes 4194320 | tf_op jit(solution)/shard_map/all_gather | solution.py:159
  884.9 4.5 fusion.8
  889.5 6.7 reduce-scatter.6.cloned.1.call-done
  896.2 1.3 fusion.20
  897.5 2.0 fusion.22
  899.6 0.3 reduce-scatter.8.cloned.1.call-start
  899.9 10.1 %all-gather.31.cloned.1.call-done = bf16[256,2048]{1,0:T(8,128)(2,1)} async-done(((bf16[128,2048]{1,0:T(8,128)(2,1)}), bf16[256,2048]{1,0:T(8,128)(2,1)}) %all-gather.31.cloned.1.call-update) | async-done | bytes 1048592 | tf_op jit(solution)/shard_map/all_gather | solution.py:22
  909.9 10.0 %convolution_multiply_fusion.1 = f32[256,3072]{1,0:T(8,128)} fusion(bf16[256,2048]{1,0:T(8,128)(2,1)} %all-gather.31.cloned.1.call-done, bf16[2048,3072]{1,0:T(8,128)(2,1)} %all-gather.15.cloned.1.call-done, f32[3072]{0:T(1024)S(1)} %copy-done.21), kind=kOutput, calls=%fused_computation.5 | convolution fusion | flops 3222011904 | bytes 16789504 | tf_op jit(solution)/shard_map/dot_general | solution.py:172
  920.0 17.0 %fusion.7 = bf16[256,2048]{1,0:T(8,128)(2,1)} fusion(bf16[3072,2048]{1,0:T(8,128)(2,1)} %all-gather.19.cloned.1.call-done, f32[2048]{0:T(1024)S(1)} %bitcast.57, bf16[256,2048]{1,0:T(8,128)(2,1)S(1)} %copy-done.19, bf16[2048,3072]{1,0:T(8,128)(2,1)} %all-gather.17.cloned.1.call-done, f32[256,3072]{1,0:T(8,128)} %convolution_multiply_fusion.1, ...), kind=kOutput, calls=%fused_computation.16 | convolution fusion | flops 6449004544 | bytes 30429184 | tf_op jit(solution)/shard_map/dot_general | solution.py:26
  937.0 9.7 %reduce-scatter.8.cloned.1.call-done = bf16[128,2048]{1,0:T(8,128)(2,1)} async-done(((bf16[256,2048]{1,0:T(8,128)(2,1)}), bf16[128,2048]{1,0:T(8,128)(2,1)}) %reduce-scatter.8.cloned.1.call-update) | async-done | bytes 524304 | tf_op jit(solution)/shard_map/reduce_scatter | solution.py:27
  946.8 2.1 fusion.23
  (93 shorter events, 0.9 us)
Async XLA Ops:
  6.5 5.9 copy-start.2
  6.5 52.5 %all-gather.13.cloned.1.call-start = ((), (), s32[]{:S(2)}) async-start(), calls=%async_computation.3 | async-start | bytes 1572864 | tf_op jit(solution)/shard_map/all_gather | solution.py:22
  9.9 6.1 copy-start.16
  10.0 167.3 %copy-start.20 = (f32[3072]{0:T(1024)S(1)}, f32[3072]{0:T(1024)}, u32[]{:S(2)}) copy-start(f32[3072]{0:T(1024)} %param.25) | copy-start | bytes 36868
  10.0 167.3 %all-gather.15.cloned.1.call-start = ((), (), s32[]{:S(2)}) async-start(), calls=%async_computation.4 | async-start | bytes 13369344 | tf_op jit(solution)/shard_map/all_gather | solution.py:132
  12.4 317.3 %all-gather.17.cloned.1.call-start = ((), (), s32[]{:S(2)}) async-start(), calls=%async_computation.5 | async-start | bytes 13369344 | tf_op jit(solution)/shard_map/all_gather | solution.py:133
  13.5 512.4 %all-gather.19.cloned.1.call-start = ((), (), s32[]{:S(2)}) async-start(), calls=%async_computation.6 | async-start | bytes 13369344 | tf_op jit(solution)/shard_map/all_gather | solution.py:137
  16.0 533.8 %reduce-scatter.4.cloned.1.call-start = ((), (), s32[]{:S(2)}) async-start(), calls=%async_computation.7 | async-start | bytes 1572864 | tf_op jit(solution)/shard_map/reduce_scatter | solution.py:27
  59.0 466.9 %copy-start.14 = (f32[16,1,128]{2,1,0:T(1,128)}, f32[16,1,128]{2,1,0:T(1,128)S(1)}, u32[]{:S(2)}) copy-start(f32[16,1,128]{2,1,0:T(1,128)S(1)} %all-gather) | copy-start | bytes 24580
  59.0 466.9 %copy-start.22 = (f32[3072]{0:T(1024)S(1)}, f32[3072]{0:T(1024)}, u32[]{:S(2)}) copy-start(f32[3072]{0:T(1024)} %param.27) | copy-start | bytes 36868
  59.0 466.9 %copy-start.18 = (bf16[256,2048]{1,0:T(8,128)(2,1)S(1)}, bf16[256,2048]{1,0:T(8,128)(2,1)}, u32[]{:S(2)}) copy-start(bf16[256,2048]{1,0:T(8,128)(2,1)} %all-gather.13.cloned.1.call-done) | copy-start | bytes 3145732
  525.9 17.2 %copy-start.6 = (f32[128,1024]{1,0:T(8,128)S(1)}, f32[128,1024]{1,0:T(8,128)}, u32[]{:S(2)}) copy-start(f32[128,1024]{1,0:T(8,128)} %param.30) | copy-start | bytes 1572868
  525.9 23.9 %copy-start = (bf16[128,2048]{1,0:T(8,128)(2,1)S(1)}, bf16[128,2048]{1,0:T(8,128)(2,1)}, u32[]{:S(2)}) copy-start(bf16[128,2048]{1,0:T(8,128)(2,1)} %param.20) | copy-start | bytes 1572868
  525.9 25.2 %copy-start.12 = (f32[2048]{0:T(1024)S(1)}, f32[2048]{0:T(1024)}, u32[]{:S(2)}) copy-start(f32[2048]{0:T(1024)} %param.22) | copy-start | bytes 24580
  543.0 9.2 copy-start.7
  543.0 10.0 %copy-start.8 = (f32[128,1024]{1,0:T(8,128)S(1)}, f32[128,1024]{1,0:T(8,128)}, u32[]{:S(2)}) copy-start(f32[128,1024]{1,0:T(8,128)} %param.34) | copy-start | bytes 1572868
  543.0 10.9 %copy-start.9 = (f32[1024,128]{1,0:T(8,128)S(1)}, f32[1024,128]{1,0:T(8,128)}, u32[]{:S(2)}) copy-start(f32[1024,128]{1,0:T(8,128)} %param.36) | copy-start | bytes 1572868
  543.0 11.7 %copy-start.17 = (f32[128]{0:T(128)S(1)}, f32[128]{0:T(128)}, u32[]{:S(2)}) copy-start(f32[128]{0:T(128)} %param.37) | copy-start | bytes 1540
  543.1 95.3 %copy-start.24 = (f32[1024]{0:T(1024)S(1)}, f32[1024]{0:T(1024)}, u32[]{:S(2)}) copy-start(f32[1024]{0:T(1024)} %param.31) | copy-start | bytes 12292
  543.1 86.1 %all-gather.25.cloned.1.call-start = ((), (), s32[]{:S(2)}) async-start(), calls=%async_computation.10 | async-start | bytes 4456448 | tf_op jit(solution)/shard_map/all_gather | solution.py:149
  543.9 94.5 %all-gather.21.cloned.1.call-start = ((), (), s32[]{:S(2)}) async-start(), calls=%async_computation.8 | async-start | bytes 1572864 | tf_op jit(solution)/shard_map/all_gather | solution.py:22
  552.2 165.8 %all-gather.27.cloned.1.call-start = ((), (), s32[]{:S(2)}) async-start(), calls=%async_computation.11 | async-start | bytes 4456448 | tf_op jit(solution)/shard_map/all_gather | solution.py:150
  553.0 242.0 %all-gather.23.cloned.1.call-start = ((), (), s32[]{:S(2)}) async-start(), calls=%async_computation.9 | async-start | bytes 4456448 | tf_op jit(solution)/shard_map/all_gather | solution.py:151
  553.9 331.1 %all-gather.29.cloned.1.call-start = ((), (), s32[]{:S(2)}) async-start(), calls=%async_computation.12 | async-start | bytes 4456448 | tf_op jit(solution)/shard_map/all_gather | solution.py:159
  554.7 341.5 %reduce-scatter.6.cloned.1.call-start = ((), (), s32[]{:S(2)}) async-start(), calls=%async_computation.13 | async-start | bytes 1572864 | tf_op jit(solution)/shard_map/reduce_scatter | solution.py:27
  598.0 120.0 %copy-start.25 = (f32[1024]{0:T(1024)S(1)}, f32[1024]{0:T(1024)}, u32[]{:S(2)}) copy-start(f32[1024]{0:T(1024)} %param.33) | copy-start | bytes 12292
  644.9 150.1 %copy-start.26 = (f32[1024]{0:T(1024)S(1)}, f32[1024]{0:T(1024)}, u32[]{:S(2)}) copy-start(f32[1024]{0:T(1024)} %param.35) | copy-start | bytes 12292
  801.0 1.5 copy-start.10
  802.8 4.0 copy-start.3
  802.8 14.4 %copy-start.4 = (bf16[256,4,128]{2,0,1:T(8,128)(2,1)}, bf16[256,4,128]{2,0,1:T(8,128)(2,1)S(1)}, u32[]{:S(2)}) copy-start(bf16[256,4,128]{2,0,1:T(8,128)(2,1)S(1)} %get-tuple-element.66) | copy-start | bytes 786436
  802.8 14.4 %copy-start.5 = (bf16[256,4,128]{2,0,1:T(8,128)(2,1)}, bf16[256,4,128]{2,0,1:T(8,128)(2,1)S(1)}, u32[]{:S(2)}) copy-start(bf16[256,4,128]{2,0,1:T(8,128)(2,1)S(1)} %get-tuple-element.67) | copy-start | bytes 786436
  817.1 5.2 copy-start.11
  884.9 12.5 %copy-start.13 = (f32[2048]{0:T(1024)S(1)}, f32[2048]{0:T(1024)}, u32[]{:S(2)}) copy-start(f32[2048]{0:T(1024)} %param.23) | copy-start | bytes 24580
  884.9 25.0 %copy-start.21 = (f32[3072]{0:T(1024)S(1)}, f32[3072]{0:T(1024)}, u32[]{:S(2)}) copy-start(f32[3072]{0:T(1024)} %param.25) | copy-start | bytes 36868
  889.4 20.5 %all-gather.31.cloned.1.call-start = ((), (), s32[]{:S(2)}) async-start(), calls=%async_computation.14 | async-start | bytes 1572864 | tf_op jit(solution)/shard_map/all_gather | solution.py:22
  899.5 20.4 %copy-start.15 = (f32[16,1,128]{2,1,0:T(1,128)S(1)}, f32[16,1,128]{2,1,0:T(1,128)}, u32[]{:S(2)}) copy-start(f32[16,1,128]{2,1,0:T(1,128)} %copy-done.14) | copy-start | bytes 24580
  899.5 20.4 %copy-start.23 = (f32[3072]{0:T(1024)S(1)}, f32[3072]{0:T(1024)}, u32[]{:S(2)}) copy-start(f32[3072]{0:T(1024)} %param.27) | copy-start | bytes 36868
  899.6 47.2 %reduce-scatter.8.cloned.1.call-start = ((), (), s32[]{:S(2)}) async-start(), calls=%async_computation.15 | async-start | bytes 1572864 | tf_op jit(solution)/shard_map/reduce_scatter | solution.py:27
  909.9 10.0 %copy-start.19 = (bf16[256,2048]{1,0:T(8,128)(2,1)S(1)}, bf16[256,2048]{1,0:T(8,128)(2,1)}, u32[]{:S(2)}) copy-start(bf16[256,2048]{1,0:T(8,128)(2,1)} %all-gather.31.cloned.1.call-done) | copy-start | bytes 3145732
  920.0 26.8 %copy-start.1 = (bf16[128,2048]{1,0:T(8,128)(2,1)S(1)}, bf16[128,2048]{1,0:T(8,128)(2,1)}, u32[]{:S(2)}) copy-start(bf16[128,2048]{1,0:T(8,128)(2,1)} %reduce-scatter.6.cloned.1.call-done) | copy-start | bytes 1572868
Sparse Core Ops, SparseCore 0:
  10.1 11.7 all-gather.12
  24.6 152.6 all-gather.14
  180.1 149.5 all-gather.16
  332.2 193.6 all-gather.18
  543.2 6.5 reduce-scatter.3
  552.4 76.7 all-gather.24
  630.8 7.6 all-gather.20
  641.2 76.7 all-gather.26
  720.8 74.1 all-gather.22
  797.5 87.3 all-gather.28
  889.6 6.5 reduce-scatter.5
  899.7 10.2 all-gather.30
  937.1 9.5 reduce-scatter.7
where the time goes:
time: 956 us; the launch traced here: 955 us
  waiting for transfers between devices  732 us (77%)
  blocking collectives  84.1 us (9%)
  matrix products  83.2 us (9%)
  other arithmetic  32.5 us (3%)
  between operations  13.6 us (1%)
    all_gather x1, waiting for transfers between devices, body(): lax.all_gather(down_weight.astype(jnp.bfloat16), 'fs', axis=1, tiled=True)  196 us
    all_gather x1, waiting for transfers between devices, body(): lax.all_gather(up_part, 'fs', axis=0, tiled=True)  142 us
    all_gather x1, waiting for transfers between devices, body(): lax.all_gather(gate_part, 'fs', axis=0, tiled=True)  118 us
    all_gather x1, waiting for transfers between devices, body(): lax.all_gather(projections[1], 'fs', axis=0, tiled=True)  73.1 us
    all_gather x1, waiting for transfers between devices, body(): lax.all_gather(projections[2], 'fs', axis=0, tiled=True)  69.6 us
    all_gather x1, waiting for transfers between devices, body(): lax.all_gather(output_weight.astype(jnp.bfloat16), 'fs', axis=1, tiled=True)  59.4 us
    all_gather x1, blocking collectives, body(): lax.all_gather(down_scale, 'fs', axis=0, tiled=True)  43 us
    all_gather x1, blocking collectives, body(): lax.all_gather(output_scale, 'fs', axis=0, tiled=True)  41.1 us
  transfers between devices with their start and end apart: 13, of which 12 were waited for; matrix products, arithmetic and copies ran while one was open for 7% of the time, Pallas kernels for 0%

commit v1 on v0

--- a/solution.py
+++ b/solution.py
@@ -10,6 +10,10 @@
 HEAD_FLOOR = 0.25
 ROTARY_BASE = 10000.0
 HIGHEST = lax.Precision.HIGHEST
+
+
+def expand_the_limits(s0):
+    return jnp.concatenate(lax.all_gather(s0, axis_name="fs"), axis=1)
 
 
 def normalize(sequence_rows, gain_vector):
@@ -134,7 +138,7 @@
     )
     gate_pre = jnp.dot(first_input, gate_full, preferred_element_type=jnp.float32)
     up_pre = jnp.dot(first_input, up_full, preferred_element_type=jnp.float32)
-    down_full = lax.all_gather(down_weight.astype(jnp.bfloat16), "fs", axis=1, tiled=True)
+    down_full = expand_the_limits(down_weight.astype(jnp.bfloat16))
     hidden_first = (jax.nn.silu(gate_pre * gate_scale) * (up_pre * up_scale)).astype(jnp.bfloat16)
     mlp_first = return_rows(hidden_first, down_full, down_factor)
     middle = (residual_in.astype(jnp.float32) + 0.5 * mlp_first).astype(jnp.bfloat16)

time: 956 us -> 905 us (0.947)
  waiting for transfers between devices: 732 us -> 670 us
  local copies, waits for them, and re-layouts: 8.91 us -> 25.6 us
    all_gather x1, waiting for transfers between devices: 196 us -> 105 us  [expand_the_limits(): return jnp.concatenate(lax.all_gather(s0, axis_name='fs'), axis=1)]
    all_gather x1, waiting for transfers between devices: 118 us -> 148 us  [body(): lax.all_gather(gate_part, 'fs', axis=0, tiled=True)]
    reshape x0 -> x1, local copies, waits for them, and re-layouts: none -> 16.7 us  [expand_the_limits(): return jnp.concatenate(lax.all_gather(s0, axis_name='fs'), axis=1)]
  transfers between devices with their start and end apart: 13 -> 13, of which waited for: 12 -> 12; matrix products, arithmetic and copies ran while one was open for 7% -> 9% of each run, Pallas kernels for 0% -> 0%
where the time goes in v1:
time: 905 us; the launch traced here: 904 us
  waiting for transfers between devices  670 us (74%)
  blocking collectives  84.6 us (9%)
  matrix products  76.9 us (8%)
  other arithmetic  32.5 us (4%)
  local copies, waits for them, and re-layouts  25.6 us (3%)
  between operations  13.6 us (2%)
    all_gather x1, waiting for transfers between devices, body(): lax.all_gather(gate_part, 'fs', axis=0, tiled=True)  148 us
    all_gather x1, waiting for transfers between devices, body(): lax.all_gather(up_part, 'fs', axis=0, tiled=True)  142 us
    all_gather x1, waiting for transfers between devices, expand_the_limits(): return jnp.concatenate(lax.all_gather(s0, axis_name='fs'), axis=1)  105 us
    all_gather x1, waiting for transfers between devices, body(): lax.all_gather(projections[1], 'fs', axis=0, tiled=True)  73.1 us
    all_gather x1, waiting for transfers between devices, body(): lax.all_gather(projections[2], 'fs', axis=0, tiled=True)  69.6 us
    all_gather x1, waiting for transfers between devices, body(): lax.all_gather(output_weight.astype(jnp.bfloat16), 'fs', axis=1, tiled=True)  59.4 us
    all_gather x1, blocking collectives, body(): lax.all_gather(down_scale, 'fs', axis=0, tiled=True)  43.4 us
    all_gather x1, blocking collectives, body(): lax.all_gather(output_scale, 'fs', axis=0, tiled=True)  41.2 us
  transfers between devices with their start and end apart: 13, of which 12 were waited for; matrix products, arithmetic and copies ran while one was open for 9% of the time, Pallas kernels for 0%

profile of v1, /device:TPU:0, one launch (start us, length us, event | category | flops | bytes accessed | tf_op | source)
XLA Modules:
  0.0 903.9 jit_solution(16825065405966446541)
XLA Ops:
  6.5 2.5 convert_element_type.122
  9.0 0.0 all-gather.14.cloned.1.call-start
  9.1 1.2 fusion.12
  10.3 2.0 fusion.14
  12.5 1.0 convert_element_type.119
  13.5 2.4 convert_element_type.120
  15.9 0.0 reduce-scatter.4.cloned.1.call-start
  16.0 43.4 %all-gather.1 = f32[16,1,128]{2,1,0:T(1,128)S(1)} all-gather(f32[1,1,128]{2,1,0:T(1,128)S(1)} %bitcast.65), channel_id=1, replica_groups=mesh['fs'=16,'tp'=2] {'fs'}, dimensions={0}, use_global_device_ids=true | all-gather | bytes 8704 | tf_op jit(solution)/shard_map/all_gather | solution.py:131
  59.5 104.9 %all-gather.32.cloned.1.call-done = bf16[49152,128]{1,0:T(8,128)(2,1)} async-done(((bf16[3072,128]{1,0:T(8,128)(2,1)}), bf16[49152,128]{1,0:T(8,128)(2,1)}) %all-gather.32.cloned.1.call-update) | async-done | bytes 12582928 | tf_op jit(solution)/shard_map/all_gather | solution.py:16
  164.3 16.7 %copy.62 = bf16[3072,16,128]{0,2,1:T(8,128)(2,1)} copy(bf16[3072,16,128]{2,0,1:T(8,128)(2,1)} %bitcast.48) | data formatting | bytes 25165824 | tf_op jit(solution)/shard_map/reshape | solution.py:16
  181.0 147.5 %all-gather.16.cloned.1.call-done = bf16[2048,3072]{1,0:T(8,128)(2,1)} async-done(((bf16[128,3072]{1,0:T(8,128)(2,1)}), bf16[2048,3072]{1,0:T(8,128)(2,1)}) %all-gather.16.cloned.1.call-update) | async-done | bytes 12582928 | tf_op jit(solution)/shard_map/all_gather | solution.py:136
  328.5 9.9 %convolution_multiply_fusion.3 = f32[256,3072]{1,0:T(8,128)} fusion(bf16[256,2048]{1,0:T(8,128)(2,1)} %all-gather.14.cloned.1.call-done, bf16[2048,3072]{1,0:T(8,128)(2,1)} %all-gather.16.cloned.1.call-done, f32[3072]{0:T(1024)S(1)} %copy-done.20), kind=kOutput, calls=%fused_computation.7 | convolution fusion | flops 3222011904 | bytes 16789504 | tf_op jit(solution)/shard_map/dot_general | solution.py:139
  338.5 142.3 %all-gather.18.cloned.1.call-done = bf16[2048,3072]{1,0:T(8,128)(2,1)} async-done(((bf16[128,3072]{1,0:T(8,128)(2,1)}), bf16[2048,3072]{1,0:T(8,128)(2,1)}) %all-gather.18.cloned.1.call-update) | async-done | bytes 12582928 | tf_op jit(solution)/shard_map/all_gather | solution.py:137
  480.8 13.8 %fusion.6 = bf16[256,2048]{1,0:T(8,128)(2,1)} fusion(bf16[3072,2048]{0,1:T(8,128)(2,1)} %bitcast.46, f32[2048]{0:T(1024)S(1)} %bitcast.63, bf16[256,2048]{1,0:T(8,128)(2,1)S(1)} %copy-done.18, bf16[2048,3072]{1,0:T(8,128)(2,1)} %all-gather.18.cloned.1.call-done, f32[256,3072]{1,0:T(8,128)} %convolution_multiply_fusion.3, f32[3072]{0:T(1024)S(1)} %copy-done.22), kind=kOutput, calls=%fused_computation.15 | convolution fusion | flops 6449004544 | bytes 30429184 | tf_op jit(solution)/shard_map/dot_general | solution.py:30
  494.7 0.7 convert_element_type.131
  495.5 5.9 reduce-scatter.4.cloned.1.call-done
  501.4 1.3 fusion.16
  502.8 1.0 fusion.18
  503.8 0.8 convert_element_type.132
  504.7 0.7 convert_element_type.128
  505.5 0.7 convert_element_type.138
  506.4 41.2 %all-gather.2 = f32[16,1,128]{2,1,0:T(1,128)S(1)} all-gather(f32[1,1,128]{2,1,0:T(1,128)S(1)} %bitcast.66), channel_id=1, replica_groups=mesh['fs'=16,'tp'=2] {'fs'}, dimensions={0}, use_global_device_ids=true | all-gather | bytes 8704 | tf_op jit(solution)/shard_map/all_gather | solution.py:132
  547.6 0.1 multiply_exponential_fusion.1
  547.7 0.7 select_multiply_fusion
  548.4 1.1 fusion.42
  549.6 31.2 %all-gather.24.cloned.1.call-done = bf16[2048,1024]{1,0:T(8,128)(2,1)} async-done(((bf16[128,1024]{1,0:T(8,128)(2,1)}), bf16[2048,1024]{1,0:T(8,128)(2,1)}) %all-gather.24.cloned.1.call-update) | async-done | bytes 4194320 | tf_op jit(solution)/shard_map/all_gather | solution.py:153
  580.8 9.2 %all-gather.20.cloned.1.call-done = bf16[256,2048]{1,0:T(8,128)(2,1)} async-done(((bf16[128,2048]{1,0:T(8,128)(2,1)}), bf16[256,2048]{1,0:T(8,128)(2,1)}) %all-gather.20.cloned.1.call-update) | async-done | bytes 1048592 | tf_op jit(solution)/shard_map/all_gather | solution.py:26
  590.0 4.7 convolution_multiply_fusion.8
  594.7 1.7 reshape.238
  596.5 73.1 %all-gather.26.cloned.1.call-done = bf16[2048,1024]{1,0:T(8,128)(2,1)} async-done(((bf16[128,1024]{1,0:T(8,128)(2,1)}), bf16[2048,1024]{1,0:T(8,128)(2,1)}) %all-gather.26.cloned.1.call-update) | async-done | bytes 4194320 | tf_op jit(solution)/shard_map/all_gather | solution.py:154
  669.6 4.7 convolution_multiply_fusion.7
  674.3 2.7 reshape.239
  677.0 69.6 %all-gather.22.cloned.1.call-done = bf16[2048,1024]{1,0:T(8,128)(2,1)} async-done(((bf16[128,1024]{1,0:T(8,128)(2,1)}), bf16[2048,1024]{1,0:T(8,128)(2,1)}) %all-gather.22.cloned.1.call-update) | async-done | bytes 4194320 | tf_op jit(solution)/shard_map/all_gather | solution.py:155
  746.6 4.6 fusion.10
  751.1 1.4 convert_element_type.130
  752.6 1.5 fusion.48
  754.1 0.3 subtract_convert_fusion.1
  754.4 3.9 fusion.27
  758.3 10.4 %while.13 = (s32[]{:T(128)}, f32[4,256,256]{2,1,0:T(8,128)S(1)}, f32[4,4,256,256]{3,2,1,0:T(8,128)}, f32[4,4,256,256]{3,2,1,0:T(8,128)}, s32[]{:T(128)}, /*index=5*/s32[]{:T(128)}, s32[]{:T(128)}) while((s32[]{:T(128)}, f32[4,256,256]{2,1,0:T(8,128)S(1)}, f32[4,4,256,256]{3,2,1,0:T(8,128)}, f32[4,4,256,256]{3,2,1,0:T(8,128)}, ...), condition=%wide.region_4.5_spmd.clone, body=%wide.region_3.4_spmd.clone.sunk | while | flops 1048603 | bytes 5243520 | solution.py:95
  758.3 1.1 bitcast_dynamic-update-slice_fusion.2
  759.4 1.5 bitcast_add_fusion.2
  760.9 1.1 bitcast_dynamic-update-slice_fusion.2
  762.0 1.5 bitcast_add_fusion.2
  763.5 1.1 bitcast_dynamic-update-slice_fusion.2
  764.6 1.5 bitcast_add_fusion.2
  766.1 1.1 bitcast_dynamic-update-slice_fusion.2
  767.2 1.5 bitcast_add_fusion.2
  768.8 5.1 fusion.24
  773.9 1.6 multiply_reduce_fusion
  775.6 0.1 copy.78
  775.7 0.3 mul.482
  776.0 0.2 copy.85
  776.2 0.7 copy.73
  776.9 0.2 copy.84
  777.1 59.4 %all-gather.28.cloned.1.call-done = bf16[1024,2048]{1,0:T(8,128)(2,1)} async-done(((bf16[1024,128]{1,0:T(8,128)(2,1)}), bf16[1024,2048]{1,0:T(8,128)(2,1)}) %all-gather.28.cloned.1.call-update) | async-done | bytes 4194320 | tf_op jit(solution)/shard_map/all_gather | solution.py:163
  836.5 4.5 fusion.8
  841.1 6.7 reduce-scatter.6.cloned.1.call-done
  847.8 1.3 fusion.20
  849.1 2.0 fusion.22
  851.2 10.3 %all-gather.30.cloned.1.call-done = bf16[256,2048]{1,0:T(8,128)(2,1)} async-done(((bf16[128,2048]{1,0:T(8,128)(2,1)}), bf16[256,2048]{1,0:T(8,128)(2,1)}) %all-gather.30.cloned.1.call-update) | async-done | bytes 1048592 | tf_op jit(solution)/shard_map/all_gather | solution.py:26
  861.5 10.0 %convolution_multiply_fusion.1 = f32[256,3072]{1,0:T(8,128)} fusion(bf16[256,2048]{1,0:T(8,128)(2,1)} %all-gather.30.cloned.1.call-done, bf16[2048,3072]{1,0:T(8,128)(2,1)} %all-gather.16.cloned.1.call-done, f32[3072]{0:T(1024)S(1)} %copy-done.21), kind=kOutput, calls=%fused_computation.5 | convolution fusion | flops 3222011904 | bytes 16789504 | tf_op jit(solution)/shard_map/dot_general | solution.py:176
  871.6 14.0 %fusion.7 = bf16[256,2048]{1,0:T(8,128)(2,1)} fusion(bf16[3072,2048]{0,1:T(8,128)(2,1)} %bitcast.47, f32[2048]{0:T(1024)S(1)} %bitcast.64, bf16[256,2048]{1,0:T(8,128)(2,1)S(1)} %copy-done.19, bf16[2048,3072]{1,0:T(8,128)(2,1)} %all-gather.18.cloned.1.call-done, f32[256,3072]{1,0:T(8,128)} %convolution_multiply_fusion.1, f32[3072]{0:T(1024)S(1)} %copy-done.23), kind=kOutput, calls=%fused_computation.16 | convolution fusion | flops 6449004544 | bytes 30429184 | tf_op jit(solution)/shard_map/dot_general | solution.py:30
  885.5 9.7 %reduce-scatter.8.cloned.1.call-done = bf16[128,2048]{1,0:T(8,128)(2,1)} async-done(((bf16[256,2048]{1,0:T(8,128)(2,1)}), bf16[128,2048]{1,0:T(8,128)(2,1)}) %reduce-scatter.8.cloned.1.call-update) | async-done | bytes 524304 | tf_op jit(solution)/shard_map/reduce_scatter | solution.py:31
  895.2 2.1 fusion.23
  (94 shorter events, 0.9 us)
Async XLA Ops:
  6.5 5.9 copy-start.2
  6.5 157.8 %all-gather.32.cloned.1.call-start = ((), (), s32[]{:S(2)}) async-start(), calls=%async_computation.15 | async-start | bytes 13369344 | tf_op jit(solution)/shard_map/all_gather | solution.py:16
  9.0 7.0 copy-start.16
  9.0 172.0 %all-gather.14.cloned.1.call-start = ((), (), s32[]{:S(2)}) async-start(), calls=%async_computation.3 | async-start | bytes 1572864 | tf_op jit(solution)/shard_map/all_gather | solution.py:26
  12.4 316.1 %all-gather.16.cloned.1.call-start = ((), (), s32[]{:S(2)}) async-start(), calls=%async_computation.4 | async-start | bytes 13369344 | tf_op jit(solution)/shard_map/all_gather | solution.py:136
  13.5 467.3 %all-gather.18.cloned.1.call-start = ((), (), s32[]{:S(2)}) async-start(), calls=%async_computation.5 | async-start | bytes 13369344 | tf_op jit(solution)/shard_map/all_gather | solution.py:137
  15.9 485.5 %reduce-scatter.4.cloned.1.call-start = ((), (), s32[]{:S(2)}) async-start(), calls=%async_computation.6 | async-start | bytes 1572864 | tf_op jit(solution)/shard_map/reduce_scatter | solution.py:31
  59.5 421.3 %copy-start.14 = (f32[16,1,128]{2,1,0:T(1,128)}, f32[16,1,128]{2,1,0:T(1,128)S(1)}, u32[]{:S(2)}) copy-start(f32[16,1,128]{2,1,0:T(1,128)S(1)} %all-gather.1) | copy-start | bytes 24580
  164.3 164.2 %copy-start.20 = (f32[3072]{0:T(1024)S(1)}, f32[3072]{0:T(1024)}, u32[]{:S(2)}) copy-start(f32[3072]{0:T(1024)} %param.25) | copy-start | bytes 36868
  181.0 299.8 %copy-start.22 = (f32[3072]{0:T(1024)S(1)}, f32[3072]{0:T(1024)}, u32[]{:S(2)}) copy-start(f32[3072]{0:T(1024)} %param.27) | copy-start | bytes 36868
  181.0 299.8 %copy-start.18 = (bf16[256,2048]{1,0:T(8,128)(2,1)S(1)}, bf16[256,2048]{1,0:T(8,128)(2,1)}, u32[]{:S(2)}) copy-start(bf16[256,2048]{1,0:T(8,128)(2,1)} %all-gather.14.cloned.1.call-done) | copy-start | bytes 3145732
  480.8 13.9 %copy-start.6 = (f32[128,1024]{1,0:T(8,128)S(1)}, f32[128,1024]{1,0:T(8,128)}, u32[]{:S(2)}) copy-start(f32[128,1024]{1,0:T(8,128)} %param.30) | copy-start | bytes 1572868
  480.8 20.6 %copy-start = (bf16[128,2048]{1,0:T(8,128)(2,1)S(1)}, bf16[128,2048]{1,0:T(8,128)(2,1)}, u32[]{:S(2)}) copy-start(bf16[128,2048]{1,0:T(8,128)(2,1)} %param.20) | copy-start | bytes 1572868
  480.8 21.9 %copy-start.12 = (f32[2048]{0:T(1024)S(1)}, f32[2048]{0:T(1024)}, u32[]{:S(2)}) copy-start(f32[2048]{0:T(1024)} %param.22) | copy-start | bytes 24580
  494.6 9.2 %copy-start.7 = (f32[128,1024]{1,0:T(8,128)S(1)}, f32[128,1024]{1,0:T(8,128)}, u32[]{:S(2)}) copy-start(f32[128,1024]{1,0:T(8,128)} %param.32) | copy-start | bytes 1572868
  494.6 10.0 %copy-start.8 = (f32[128,1024]{1,0:T(8,128)S(1)}, f32[128,1024]{1,0:T(8,128)}, u32[]{:S(2)}) copy-start(f32[128,1024]{1,0:T(8,128)} %param.34) | copy-start | bytes 1572868
  494.6 10.9 %copy-start.9 = (f32[1024,128]{1,0:T(8,128)S(1)}, f32[1024,128]{1,0:T(8,128)}, u32[]{:S(2)}) copy-start(f32[1024,128]{1,0:T(8,128)} %param.36) | copy-start | bytes 1572868
  494.6 11.7 %copy-start.17 = (f32[128]{0:T(128)S(1)}, f32[128]{0:T(128)}, u32[]{:S(2)}) copy-start(f32[128]{0:T(128)} %param.37) | copy-start | bytes 1540
  494.7 95.4 %copy-start.24 = (f32[1024]{0:T(1024)S(1)}, f32[1024]{0:T(1024)}, u32[]{:S(2)}) copy-start(f32[1024]{0:T(1024)} %param.31) | copy-start | bytes 12292
  494.7 86.1 %all-gather.24.cloned.1.call-start = ((), (), s32[]{:S(2)}) async-start(), calls=%async_computation.9 | async-start | bytes 4456448 | tf_op jit(solution)/shard_map/all_gather | solution.py:153
  495.5 94.5 %all-gather.20.cloned.1.call-start = ((), (), s32[]{:S(2)}) async-start(), calls=%async_computation.7 | async-start | bytes 1572864 | tf_op jit(solution)/shard_map/all_gather | solution.py:26
  503.8 165.8 %all-gather.26.cloned.1.call-start = ((), (), s32[]{:S(2)}) async-start(), calls=%async_computation.10 | async-start | bytes 4456448 | tf_op jit(solution)/shard_map/all_gather | solution.py:154
  504.6 242.0 %all-gather.22.cloned.1.call-start = ((), (), s32[]{:S(2)}) async-start(), calls=%async_computation.8 | async-start | bytes 4456448 | tf_op jit(solution)/shard_map/all_gather | solution.py:155
  505.5 331.1 %all-gather.28.cloned.1.call-start = ((), (), s32[]{:S(2)}) async-start(), calls=%async_computation.11 | async-start | bytes 4456448 | tf_op jit(solution)/shard_map/all_gather | solution.py:163
  506.3 341.5 %reduce-scatter.6.cloned.1.call-start = ((), (), s32[]{:S(2)}) async-start(), calls=%async_computation.12 | async-start | bytes 1572864 | tf_op jit(solution)/shard_map/reduce_scatter | solution.py:31
  549.6 120.0 %copy-start.25 = (f32[1024]{0:T(1024)S(1)}, f32[1024]{0:T(1024)}, u32[]{:S(2)}) copy-start(f32[1024]{0:T(1024)} %param.33) | copy-start | bytes 12292
  596.4 150.1 %copy-start.26 = (f32[1024]{0:T(1024)S(1)}, f32[1024]{0:T(1024)}, u32[]{:S(2)}) copy-start(f32[1024]{0:T(1024)} %param.35) | copy-start | bytes 12292
  752.6 1.5 copy-start.10
  754.4 4.0 copy-start.3
  754.4 14.4 %copy-start.4 = (bf16[256,4,128]{2,0,1:T(8,128)(2,1)}, bf16[256,4,128]{2,0,1:T(8,128)(2,1)S(1)}, u32[]{:S(2)}) copy-start(bf16[256,4,128]{2,0,1:T(8,128)(2,1)S(1)} %get-tuple-element.66) | copy-start | bytes 786436
  754.4 14.4 %copy-start.5 = (bf16[256,4,128]{2,0,1:T(8,128)(2,1)}, bf16[256,4,128]{2,0,1:T(8,128)(2,1)S(1)}, u32[]{:S(2)}) copy-start(bf16[256,4,128]{2,0,1:T(8,128)(2,1)S(1)} %get-tuple-element.67) | copy-start | bytes 786436
  768.7 5.2 copy-start.11
  836.5 12.5 %copy-start.13 = (f32[2048]{0:T(1024)S(1)}, f32[2048]{0:T(1024)}, u32[]{:S(2)}) copy-start(f32[2048]{0:T(1024)} %param.23) | copy-start | bytes 24580
  836.5 25.0 %copy-start.21 = (f32[3072]{0:T(1024)S(1)}, f32[3072]{0:T(1024)}, u32[]{:S(2)}) copy-start(f32[3072]{0:T(1024)} %param.25) | copy-start | bytes 36868
  841.0 20.5 %all-gather.30.cloned.1.call-start = ((), (), s32[]{:S(2)}) async-start(), calls=%async_computation.13 | async-start | bytes 1572864 | tf_op jit(solution)/shard_map/all_gather | solution.py:26
  851.1 20.4 %copy-start.15 = (f32[16,1,128]{2,1,0:T(1,128)S(1)}, f32[16,1,128]{2,1,0:T(1,128)}, u32[]{:S(2)}) copy-start(f32[16,1,128]{2,1,0:T(1,128)} %copy-done.14) | copy-start | bytes 24580
  851.1 20.4 %copy-start.23 = (f32[3072]{0:T(1024)S(1)}, f32[3072]{0:T(1024)}, u32[]{:S(2)}) copy-start(f32[3072]{0:T(1024)} %param.27) | copy-start | bytes 36868
  851.1 44.1 %reduce-scatter.8.cloned.1.call-start = ((), (), s32[]{:S(2)}) async-start(), calls=%async_computation.14 | async-start | bytes 1572864 | tf_op jit(solution)/shard_map/reduce_scatter | solution.py:31
  861.5 10.0 %copy-start.19 = (bf16[256,2048]{1,0:T(8,128)(2,1)S(1)}, bf16[256,2048]{1,0:T(8,128)(2,1)}, u32[]{:S(2)}) copy-start(bf16[256,2048]{1,0:T(8,128)(2,1)} %all-gather.30.cloned.1.call-done) | copy-start | bytes 3145732
  871.5 23.7 %copy-start.1 = (bf16[128,2048]{1,0:T(8,128)(2,1)S(1)}, bf16[128,2048]{1,0:T(8,128)(2,1)}, u32[]{:S(2)}) copy-start(bf16[128,2048]{1,0:T(8,128)(2,1)} %reduce-scatter.6.cloned.1.call-done) | copy-start | bytes 1572868
Sparse Core Ops, SparseCore 0:
  10.1 154.1 all-gather.31
  165.9 7.1 all-gather.13
  175.9 152.5 all-gather.15
  331.2 149.5 all-gather.17
  494.8 6.5 reduce-scatter.3
  504.0 76.7 all-gather.23
  582.4 7.6 all-gather.19
  592.8 76.7 all-gather.25
  672.4 74.1 all-gather.21
  749.1 87.3 all-gather.27
  841.1 6.5 reduce-scatter.5
  851.2 10.2 all-gather.29
  885.7 9.5 reduce-scatter.7
